TPU v7x, 256 devices: a whole 4x4x8 slice. The times are simulated.
256 devices in a mesh: sp: 64 (over z, y, core), tp: 4 (over x).
Axes of the slice: x: 4, y: 4, z: 8, core: 2. Of those that a mesh axis runs over, the one named last changes fastest.
Arguments:
- stream: bfloat16 [32768, 2048], P(('sp', 'tp')), may hold values from -6 to 6
- conv_value: bfloat16 [32768, 512], P('sp', 'tp'), may hold values from -6 to 6
- conv_gate: bfloat16 [32768, 512], P('sp', 'tp'), may hold values from -8 to 8
- doc_ids: int32 [32768], P('sp'), may hold values from 0 to 31, never falling along the last dimension, each value on 1 to 2048 neighbouring positions
- conv_taps: float32 [31, 512], P(None, 'tp'), may hold values from -2.2 to 2.2
- conv_bias: float32 [512], P('tp'), may hold values from -3 to 3
- chan_gain: float32 [512], replicated, may hold values from 0.1 to 1.9
- chan_shift: float32 [512], replicated, may hold values from -3 to 3
- out_weight: bfloat16 [512, 2048], replicated, may hold values from -0.25 to 0.25
- rms_gain: float32 [2048], replicated, may hold values from 0.1 to 1.9
- expert_ids: int32 [32768, 2], P(('sp', 'tp')), may hold values from 0 to 127, all different within a row; in each aligned block of 128 rows (0 to 127, 128 to 255, ...) at most 3 rows name the same one
- group_prob: float32 [32768], P(('sp', 'tp')), may hold values from 0.3 to 1
- route_logits: float32 [32768, 2], P(('sp', 'tp')), may hold values from -6 to 6
- expert_gate: bfloat16 [128, 2048, 1024], P('sp', None, 'tp'), may hold values from -0.125 to 0.125
- expert_up: bfloat16 [128, 2048, 1024], P('sp', None, 'tp'), may hold values from -0.125 to 0.125
- expert_down: bfloat16 [128, 1024, 2048], P('sp', 'tp'), may hold values from -0.1875 to 0.1875
Outputs:
- mixed: bfloat16 [32768, 2048], P(('sp', 'tp'))
Inputs may be any that keep to these rules, and one draw needn't show every extreme that they name: `expert_ids`: each row names 2 different experts. In each aligned block of 128 rows (the rows of one device) no expert is named by more than 3 rows, a bound that some block reaches. `doc_ids`: document numbers never fall along the sequence; every document has 1 to 2048 positions, one exactly 2048.
All inputs are finite; a program needn't handle non-finite values.
Results may differ from a plain program's by a relative error of at most 0.012.
Values may be sent and summed in bfloat16 or wider, within the bound.
A program may use at most 64 MiB of HBM per device.

v0:
```python
import jax
import jax.numpy as jnp
from jax import lax
from jax.sharding import PartitionSpec as P

eps = 1e-06


def passed_along(x, axis, by):
    size = lax.axis_size(axis)
    pairs = [(i, i + by) for i in range(size) if 0 <= i + by < size]
    return lax.ppermute(x, axis, pairs)


def causal_conv(values, gates, docs, conv_taps, conv_bias):
    reach = conv_taps.shape[0] - 1
    acts = values.astype(jnp.float32) * jax.nn.sigmoid(gates.astype(jnp.float32))
    total = values.shape[0] - reach
    result = jnp.broadcast_to(conv_bias[None, :], (total, values.shape[1]))
    own_doc = docs[reach:]
    for offset in range(reach + 1):
        begin = reach - offset
        same = (docs[begin : begin + total] == own_doc)[:, None]
        result = (
            result + jnp.where(same, acts[begin : begin + total], 0.0) * conv_taps[offset][None, :]
        )
    return result.astype(jnp.bfloat16)


def finish_norm(values, mean, square, gain, shift):
    spread = square - mean * mean
    scaled = (values - mean) * lax.rsqrt(spread + eps) * gain + shift
    return jax.nn.silu(scaled).astype(jnp.bfloat16)


def apply_experts(arrived, expert_gate, expert_up, expert_down):
    outputs = []
    for local in range(arrived.shape[1]):
        rows = arrived[:, local].reshape(-1, arrived.shape[3])
        gated = jnp.dot(rows, expert_gate[local], preferred_element_type=jnp.float32)
        upward = jnp.dot(rows, expert_up[local], preferred_element_type=jnp.float32)
        hidden = (jax.nn.silu(gated) * upward).astype(jnp.bfloat16)
        partial_value = jnp.dot(hidden, expert_down[local], preferred_element_type=jnp.float32)
        outputs.append(partial_value.reshape(arrived.shape[0], arrived.shape[2], arrived.shape[3]))
    return jnp.stack(outputs, axis=1)


def split_quarters(partial_value, quarters):
    shape = partial_value.shape
    return partial_value.astype(jnp.bfloat16).reshape(
        shape[0], shape[1], quarters, shape[2] // quarters, shape[3]
    )


def body(
    stream,
    conv_value,
    conv_gate,
    doc_ids,
    conv_taps,
    conv_bias,
    chan_gain,
    chan_shift,
    out_weight,
    rms_gain,
    expert_ids,
    group_prob,
    route_logits,
    expert_gate,
    expert_up,
    expert_down,
):
    reach = conv_taps.shape[0] - 1
    tail_value, tail_gate, tail_doc = passed_along(
        (conv_value[-reach:], conv_gate[-reach:], doc_ids[-reach:]), "sp", 1
    )
    values = jnp.concatenate([tail_value, conv_value], axis=0)
    gates = jnp.concatenate([tail_gate, conv_gate], axis=0)
    docs = jnp.concatenate([tail_doc, doc_ids], axis=0)
    conved = causal_conv(values, gates, docs, conv_taps, conv_bias)
    own_rows = stream.shape[0]
    regrouped = lax.all_to_all(conved, "tp", split_axis=0, concat_axis=1, tiled=True)
    floats = regrouped.astype(jnp.float32)
    mean = jnp.mean(floats, axis=-1, keepdims=True)
    square = jnp.mean(floats * floats, axis=-1, keepdims=True)
    activated = finish_norm(floats, mean, square, chan_gain, chan_shift)
    projected = jnp.dot(activated, out_weight, preferred_element_type=jnp.float32)
    resid = (stream.astype(jnp.float32) + projected).astype(jnp.bfloat16)
    resid_float = resid.astype(jnp.float32)
    mean_square = jnp.mean(resid_float * resid_float, axis=-1, keepdims=True)
    normed = (resid_float * lax.rsqrt(mean_square + eps) * rms_gain).astype(jnp.bfloat16)
    gap = route_logits[:, 0] - route_logits[:, 1]
    weights = jnp.stack(
        [group_prob * jax.nn.sigmoid(gap), group_prob * jax.nn.sigmoid(-gap)], axis=1
    )
    sp_count = lax.axis_size("sp")
    tp_count = lax.axis_size("tp")
    local_experts = expert_gate.shape[0]
    experts_all = sp_count * local_experts
    top_count = expert_ids.shape[1]
    capacity = max(2, 3 * own_rows * top_count // (2 * experts_all))
    flat_ids = expert_ids.reshape(-1)
    onehot = (flat_ids[:, None] == jnp.arange(experts_all, dtype=jnp.int32)[None, :]).astype(
        jnp.int32
    )
    earlier = jnp.cumsum(onehot, axis=0) - onehot
    ranks = jnp.sum(earlier * onehot, axis=1)
    dest = flat_ids * capacity + ranks
    route_token = jnp.arange(flat_ids.shape[0], dtype=jnp.int32) // top_count
    source = jnp.full((experts_all * capacity,), own_rows, jnp.int32).at[dest].set(route_token)
    with_blank = jnp.concatenate([normed, jnp.zeros((1, normed.shape[1]), jnp.bfloat16)], axis=0)
    outgoing = with_blank[source].reshape(sp_count, local_experts, capacity, normed.shape[1])
    arrived_own = lax.all_to_all(outgoing, "sp", split_axis=0, concat_axis=0, tiled=True)
    arrived = lax.all_gather(arrived_own, "tp", axis=2, tiled=True)
    partial_value = apply_experts(arrived, expert_gate, expert_up, expert_down)
    quarters = lax.all_to_all(
        split_quarters(partial_value, tp_count), "tp", split_axis=2, concat_axis=2, tiled=True
    )
    summed = jnp.sum(quarters.astype(jnp.float32), axis=2).astype(jnp.bfloat16)
    routed = lax.all_to_all(summed, "sp", split_axis=0, concat_axis=0, tiled=True)
    flat_out = routed.reshape(experts_all * capacity, normed.shape[1])
    picked = flat_out[dest].reshape(own_rows, top_count, normed.shape[1]).astype(jnp.float32)
    combined = jnp.sum(weights[:, :, None] * picked, axis=1)
    return (resid_float + combined).astype(jnp.bfloat16)


def solution(mesh):
    placed = (
        P(("sp", "tp"), None),
        P("sp", "tp"),
        P("sp", "tp"),
        P("sp"),
        P(None, "tp"),
        P("tp"),
        P(),
        P(),
        P(),
        P(),
        P(("sp", "tp"), None),
        P(("sp", "tp")),
        P(("sp", "tp"), None),
        P("sp", None, "tp"),
        P("sp", None, "tp"),
        P("sp", "tp", None),
    )
    return jax.shard_map(
        body, mesh=mesh, in_specs=placed, out_specs=P(("sp", "tp"), None), check_vma=False
    )
```

profile of v0, /device:TPU:1, one launch (start us, length us, event | category | flops | bytes accessed | tf_op | source)
XLA Modules:
  0.0 369.9 jit_solution(13380096626957042728)
XLA Ops:
  6.5 0.9 slice.325
  7.5 4.6 %collective-permute-start.2 = (s32[30]{0:T(128)S(1)}, s32[30]{0:T(128)S(1)}, u32[]{:S(2)}, u32[]{:S(2)}) collective-permute-start(s32[30]{0:T(128)S(1)} %slice.325), channel_id=1, source_target_pairs={{0,4},{4,8},{8,12},{12,16},{16,20},{20,24},{24,28},{28,32},{32,36}... | collective-permute-start | bytes 368 | tf_op jit(solution)/shard_map/ppermute | solution.py:12
  12.0 0.7 slice.321
  12.7 1.9 collective-permute-start
  14.7 0.7 slice.322
  15.4 3.6 collective-permute-start.1
  18.9 1.0 slice_bitcast_fusion.31
  20.0 1.0 slice_bitcast_fusion.30
  20.9 0.8 copy.40
  21.7 0.1 eq.149
  21.8 0.1 eq.145
  22.0 0.7 broadcast_multiply_fusion
  22.8 0.2 fusion.88
  23.1 0.1 copy.39
  23.2 0.1 mul.522
  23.3 0.2 fusion.90
  23.5 1.4 scatter_custom_fusion
  25.0 0.8 pad_add_fusion
  25.7 0.8 slice_compare_fusion.29
  26.5 0.8 slice_compare_fusion.28
  27.3 1.1 divide_multiply_fusion
  28.4 3.4 fusion.25
  31.8 4.0 %all-to-all-start = ((bf16[4,128,128]{2,1,0:T(8,128)(2,1)}), bf16[4,128,128]{2,1,0:T(8,128)(2,1)S(1)}, u32[]{:S(2)}, u32[]{:S(2)}) async-start(bf16[4,128,128]{2,1,0:T(8,128)(2,1)} %bitcast.31), calls=%async_computation | async-start | bytes 262144 | tf_op jit(solution)/shard_map/all_to_all | solution.py:82
  35.9 5.1 %all-to-all-done = bf16[4,128,128]{2,1,0:T(8,128)(2,1)S(1)} async-done(((bf16[4,128,128]{2,1,0:T(8,128)(2,1)}), bf16[4,128,128]{2,1,0:T(8,128)(2,1)S(1)}, u32[]{:S(2)}, u32[]{:S(2)}) %all-to-all-start) | async-done | bytes 131104 | tf_op jit(solution)/shard_map/all_to_all | solution.py:82
  41.0 0.1 copy.37
  41.1 0.1 convert_reduce_fusion
  41.3 0.2 multiply_convert_fusion.1
  41.5 1.6 multiply_reduce_fusion.1
  43.1 0.2 multiply_convert_fusion
  43.3 3.1 gather_fusion
  46.5 4.0 %reshape.161 = bf16[64,2,3,2048]{3,2,1,0:T(4,128)(2,1)S(1)} reshape(bf16[384,2048]{1,0:T(8,128)(2,1)} %gather_fusion) | data formatting | bytes 3145728 | tf_op jit(solution)/shard_map/reshape | solution.py:112
  50.5 2.1 copy.44
  52.6 50.4 %all_to_all.28 = bf16[64,2,3,2048]{3,1,2,0:T(2,128)(2,1)S(1)} all-to-all(bf16[64,2,3,2048]{3,1,2,0:T(2,128)(2,1)S(1)} %copy.44), channel_id=1, replica_groups=mesh['sp'=64,'tp'=4] {'sp'}, dimensions={0} | all-to-all | bytes 3145728 | tf_op jit(solution)/shard_map/all_to_all | solution.py:113
  103.0 1.8 copy.45
  104.8 63.3 %all-gather.2.cloned.1.call-done = bf16[64,2,12,2048]{3,0,1,2:T(8,128)(2,1)} async-done(((bf16[64,2,3,2048]{3,0,1,2:T(8,128)(2,1)}), bf16[64,2,12,2048]{3,0,1,2:T(8,128)(2,1)}) %all-gather.2.cloned.1.call-update) | async-done | bytes 6291472 | tf_op jit(solution)/shard_map/all_gather | solution.py:114
  168.1 5.3 %fusion.97 = (bf16[64,1,12,2048]{3,0,1,2:T(8,128)(2,1)S(1)}, bf16[64,1,12,2048]{3,0,1,2:T(8,128)(2,1)}) fusion(bf16[64,2,12,2048]{3,0,1,2:T(8,128)(2,1)} %all-gather.2.cloned.1.call-done), kind=kLoop, calls=%fused_computation.230 | loop fusion | bytes 12582912 | tf_op jit(solution)/shard_map/slice | solution.py:39
  173.5 3.7 %copy.46 = bf16[64,1,12,2048]{3,2,0,1:T(8,128)(2,1)} copy(bf16[64,1,12,2048]{3,0,1,2:T(8,128)(2,1)S(1)} %get-tuple-element.7) | data formatting | bytes 6291456 | tf_op jit(solution)/shard_map/slice | solution.py:39
  177.2 6.3 %reshape_squeeze.6 = bf16[768,2048]{1,0:T(8,128)(2,1)} reshape(bf16[64,1,12,2048]{3,2,0,1:T(8,128)(2,1)} %copy.46) | data formatting | bytes 6291456 | tf_op jit(solution)/shard_map/reshape;squeeze | solution.py:39
  183.5 3.0 fusion.12
  186.6 0.4 copy-done.14
  187.0 1.0 fusion.4
  188.0 1.0 reshape.162
  189.0 5.6 %copy.48 = bf16[64,1,12,2048]{3,2,0,1:T(8,128)(2,1)} copy(bf16[64,1,12,2048]{3,0,1,2:T(8,128)(2,1)} %get-tuple-element.8) | data formatting | bytes 6291456 | tf_op jit(solution)/shard_map/slice | solution.py:39
  194.6 6.3 %reshape_squeeze.7 = bf16[768,2048]{1,0:T(8,128)(2,1)} reshape(bf16[64,1,12,2048]{3,2,0,1:T(8,128)(2,1)} %copy.48) | data formatting | bytes 6291456 | tf_op jit(solution)/shard_map/reshape;squeeze | solution.py:39
  201.0 3.0 fusion.9
  204.0 0.4 copy-done.15
  204.4 1.7 fusion.5
  206.2 2.1 reshape.163
  208.2 2.1 fusion
  210.4 1.0 fusion.1
  211.4 0.6 pad_maximum_fusion
  211.9 1.1 copy.50
  213.1 73.9 %all_to_all.29 = bf16[64,2,4,3,2048]{4,0,3,1,2:T(8,128)(2,1)} all-to-all(bf16[64,2,4,3,2048]{4,0,3,1,2:T(8,128)(2,1)S(1)} %copy.50), channel_id=1, replica_groups=mesh['sp'=64,'tp'=4] {'tp'}, dimensions={2} | all-to-all | bytes 12582912 | tf_op jit(solution)/shard_map/all_to_all | solution.py:116
  287.0 4.2 %reduce_sum.64 = bf16[64,2,3,2048]{3,0,2,1:T(8,128)(2,1)S(1)} reduce(bf16[64,2,4,3,2048]{4,0,3,1,2:T(8,128)(2,1)} %all_to_all.29, bf16[]{:T(256)} %constant.46.clone.1), dimensions={2}, to_apply=%region_7.8 | reduce | flops 2359296 | bytes 7864322 | tf_op jit(solution)/shard_map/reduce_sum | solution.py:119
  291.2 2.8 copy.52
  293.9 12.1 %all-to-all-start.3 = ((bf16[64,2,3,2048]{3,1,2,0:T(2,128)(2,1)}), bf16[64,2,3,2048]{3,1,2,0:T(2,128)(2,1)S(1)}, u32[]{:S(2)}, u32[]{:S(2)}) async-start(bf16[64,2,3,2048]{3,1,2,0:T(2,128)(2,1)} %copy.52), calls=%async_computation.3 | async-start | bytes 3145728 | tf_op jit(solution)/shard_map/all_to_all | solution.py:120
  306.1 0.1 copy.38
  306.2 38.9 %all-to-all-done.3 = bf16[64,2,3,2048]{3,1,2,0:T(2,128)(2,1)S(1)} async-done(((bf16[64,2,3,2048]{3,1,2,0:T(2,128)(2,1)}), bf16[64,2,3,2048]{3,1,2,0:T(2,128)(2,1)S(1)}, u32[]{:S(2)}, u32[]{:S(2)}) %all-to-all-start.3) | async-done | bytes 1572896 | tf_op jit(solution)/shard_map/all_to_all | solution.py:120
  345.1 2.4 copy.53
  347.5 3.9 %reshape.164 = bf16[384,2048]{1,0:T(8,128)(2,1)S(1)} reshape(bf16[64,2,3,2048]{3,2,1,0:T(4,128)(2,1)} %copy.53) | data formatting | bytes 3145728 | tf_op jit(solution)/shard_map/reshape | solution.py:121
  351.4 2.3 gather_fusion.1
  353.8 3.4 reshape.168
  357.1 5.0 %multiply_reduce_fusion = f32[128,2048]{1,0:T(8,128)S(1)} fusion(f32[128,2,2048]{2,1,0:T(2,128)} %reshape.168, f32[128,2]{1,0:T(8,128)S(1)} %copy.38), kind=kLoop, calls=%fused_computation.11 | loop fusion | flops 786432 | bytes 3146752 | tf_op jit(solution)/shard_map/reduce_sum | solution.py:123
  362.1 0.9 add_convert_fusion
  (53 shorter events, 0.4 us)
Async XLA Ops:
  6.5 35.0 %copy-start = (bf16[512,2048]{1,0:T(8,128)(2,1)S(1)}, bf16[512,2048]{1,0:T(8,128)(2,1)}, u32[]{:S(2)}) copy-start(bf16[512,2048]{1,0:T(8,128)(2,1)} %param.24) | copy-start | bytes 6291460
  6.5 21.8 %copy-start.11 = (f32[128]{0:T(128)S(1)}, f32[128]{0:T(128)}, u32[]{:S(2)}) copy-start(f32[128]{0:T(128)} %param.21) | copy-start | bytes 1540
  7.5 17.5 %collective-permute-start.2 = (s32[30]{0:T(128)S(1)}, s32[30]{0:T(128)S(1)}, u32[]{:S(2)}, u32[]{:S(2)}) collective-permute-start(s32[30]{0:T(128)S(1)} %slice.325), channel_id=1, source_target_pairs={{0,4},{4,8},{8,12},{12,16},{16,20},{20,24},{24,28},{28,32},{32,36}... | collective-permute-start | bytes 368 | tf_op jit(solution)/shard_map/ppermute | solution.py:12
  12.7 14.5 %collective-permute-start = (bf16[30,128]{1,0:T(8,128)(2,1)S(1)}, bf16[30,128]{1,0:T(8,128)(2,1)S(1)}, u32[]{:S(2)}, u32[]{:S(2)}) collective-permute-start(bf16[30,128]{1,0:T(8,128)(2,1)S(1)} %slice.321), channel_id=1, source_target_pairs={{0,4},{4,8},{8,12},{12,16},{16,20},{20,24},{24,28},{28,32},{32,36}... | collective-permute-start | bytes 23048 | tf_op jit(solution)/shard_map/ppermute | solution.py:12
  15.4 11.9 %collective-permute-start.1 = (bf16[30,128]{1,0:T(8,128)(2,1)S(1)}, bf16[30,128]{1,0:T(8,128)(2,1)S(1)}, u32[]{:S(2)}, u32[]{:S(2)}) collective-permute-start(bf16[30,128]{1,0:T(8,128)(2,1)S(1)} %slice.322), channel_id=1, source_target_pairs={{0,4},{4,8},{8,12},{12,16},{16,20},{20,24},{24,28},{28,32},{32,36}... | collective-permute-start | bytes 23048 | tf_op jit(solution)/shard_map/ppermute | solution.py:12
  28.4 12.9 %copy-start.7 = (f32[512]{0:T(512)S(1)}, f32[512]{0:T(512)}, u32[]{:S(2)}) copy-start(f32[512]{0:T(512)} %param.23) | copy-start | bytes 6148
  28.4 12.9 %copy-start.8 = (f32[512]{0:T(512)S(1)}, f32[512]{0:T(512)}, u32[]{:S(2)}) copy-start(f32[512]{0:T(512)} %param.22) | copy-start | bytes 6148
  31.8 9.1 %all-to-all-start = ((bf16[4,128,128]{2,1,0:T(8,128)(2,1)}), bf16[4,128,128]{2,1,0:T(8,128)(2,1)S(1)}, u32[]{:S(2)}, u32[]{:S(2)}) async-start(bf16[4,128,128]{2,1,0:T(8,128)(2,1)} %bitcast.31), calls=%async_computation | async-start | bytes 262144 | tf_op jit(solution)/shard_map/all_to_all | solution.py:82
  35.9 132.3 %all-gather.2.cloned.1.call-start = ((), (), s32[]{:S(2)}) async-start(), calls=%async_computation.4 | async-start | bytes 7864320 | tf_op jit(solution)/shard_map/all_gather | solution.py:114
  41.3 1.9 copy-start.6
  177.2 6.3 %copy-start.12 = (bf16[2,2048,256]{2,1,0:T(8,128)(2,1)S(1)}, bf16[2,2048,256]{2,1,0:T(8,128)(2,1)}, u32[]{:S(2)}) copy-start(bf16[2,2048,256]{2,1,0:T(8,128)(2,1)} %param.29) | copy-start | bytes 6291460
  183.5 3.0 copy-start.2
  183.5 3.5 copy-start.14
  194.6 6.3 %copy-start.13 = (bf16[2,2048,256]{2,1,0:T(8,128)(2,1)S(1)}, bf16[2,2048,256]{2,1,0:T(8,128)(2,1)}, u32[]{:S(2)}) copy-start(bf16[2,2048,256]{2,1,0:T(8,128)(2,1)} %param.29) | copy-start | bytes 6291460
  200.9 3.0 copy-start.3
  201.0 3.5 copy-start.15
  204.4 3.8 %copy-start.4 = (bf16[2,256,2048]{2,1,0:T(8,128)(2,1)S(1)}, bf16[2,256,2048]{2,1,0:T(8,128)(2,1)}, u32[]{:S(2)}) copy-start(bf16[2,256,2048]{2,1,0:T(8,128)(2,1)} %param.31) | copy-start | bytes 6291460
  208.2 2.1 copy-start.5
  293.9 12.1 %copy-start.9 = (f32[128,2]{0,1:T(2,128)S(1)}, f32[128,2]{0,1:T(2,128)}, u32[]{:S(2)}) copy-start(f32[128,2]{0,1:T(2,128)} %param.28) | copy-start | bytes 3076
  293.9 12.1 %copy-start.10 = (f32[128]{0:T(128)S(1)}, f32[128]{0:T(128)}, u32[]{:S(2)}) copy-start(f32[128]{0:T(128)} %param.27) | copy-start | bytes 1540
  293.9 51.1 %all-to-all-start.3 = ((bf16[64,2,3,2048]{3,1,2,0:T(2,128)(2,1)}), bf16[64,2,3,2048]{3,1,2,0:T(2,128)(2,1)S(1)}, u32[]{:S(2)}, u32[]{:S(2)}) async-start(bf16[64,2,3,2048]{3,1,2,0:T(2,128)(2,1)} %copy.52), calls=%async_computation.3 | async-start | bytes 3145728 | tf_op jit(solution)/shard_map/all_to_all | solution.py:120
  357.1 5.9 %copy-start.1 = (bf16[512,2048]{1,0:T(8,128)(2,1)S(1)}, bf16[512,2048]{1,0:T(8,128)(2,1)}, u32[]{:S(2)}) copy-start(bf16[512,2048]{1,0:T(8,128)(2,1)} %param.24) | copy-start | bytes 6291460
Sparse Core Ops, SparseCore 0:
  104.9 63.1 all-gather.1
where the time goes:
time: 371 us; the launch traced here: 370 us
  blocking collectives  124 us (33%)
  waiting for transfers between devices  107 us (29%)
  local copies, waits for them, and re-layouts  65.7 us (18%)
  starting transfers between devices  26.1 us (7%)
  other arithmetic  19.2 us (5%)
  between operations  13.8 us (4%)
  matrix products  13.4 us (4%)
    all_to_all x1, blocking collectives, body(): lax.all_to_all(split_quarters(partial_value, tp_count), 'tp', split_axis=...  73.9 us
    all_gather x1, waiting for transfers between devices, body(): arrived = lax.all_gather(arrived_own, 'tp', axis=2, tiled=True)  63.3 us
    all_to_all x1, blocking collectives, body(): lax.all_to_all(outgoing, 'sp', split_axis=0, concat_axis=0, tiled=True)  50.4 us
    all_to_all x1, waiting for transfers between devices, body(): lax.all_to_all(summed, 'sp', split_axis=0, concat_axis=0, tiled=True)  38.9 us
    slice x3, local copies, waits for them, and re-layouts, apply_experts(): rows = arrived[:, local].reshape(-1, arrived.shape[3])  14.7 us
    another operation x2, local copies, waits for them, and re-layouts, apply_experts(): rows = arrived[:, local].reshape(-1, arrived.shape[3])  12.6 us
    all_to_all x1, starting transfers between devices, body(): lax.all_to_all(summed, 'sp', split_axis=0, concat_axis=0, tiled=True)  12.1 us
    ppermute x3, starting transfers between devices, passed_along(): return lax.ppermute(x, axis, pairs)  10.1 us
  transfers between devices with their start and end apart: 6, of which 3 were waited for; matrix products, arithmetic and copies ran while one was open for 3% of the time, Pallas kernels for 0%

commit v1 on v0

--- a/solution.py
+++ b/solution.py
@@ -111,7 +111,9 @@
     with_blank = jnp.concatenate([normed, jnp.zeros((1, normed.shape[1]), jnp.bfloat16)], axis=0)
     outgoing = with_blank[source].reshape(sp_count, local_experts, capacity, normed.shape[1])
     arrived_own = lax.all_to_all(outgoing, "sp", split_axis=0, concat_axis=0, tiled=True)
-    arrived = lax.all_gather(arrived_own, "tp", axis=2, tiled=True)
+    arrived = jnp.concatenate(
+        lax.all_to_all(jnp.stack([arrived_own] * lax.axis_size("tp")), "tp", 0, 0), axis=2
+    )
     partial_value = apply_experts(arrived, expert_gate, expert_up, expert_down)
     quarters = lax.all_to_all(
         split_quarters(partial_value, tp_count), "tp", split_axis=2, concat_axis=2, tiled=True

time: 371 us -> 362 us (0.976)
  blocking collectives: 124 us -> 195 us
  waiting for transfers between devices: 107 us -> 44 us
  between operations: 13.8 us -> 0.44 us
    all_to_all x0 -> x1, blocking collectives: none -> 72.2 us  [body(): lax.all_to_all(jnp.stack([arrived_own] * lax.axis_size('tp')), 'tp', 0, 0)]
    all_gather x1 -> x0, waiting for transfers between devices: 63.3 us -> none  [body(): arrived = lax.all_gather(arrived_own, 'tp', axis=2, tiled=True)]
  transfers between devices with their start and end apart: 6 -> 5, of which waited for: 3 -> 2; matrix products, arithmetic and copies ran while one was open for 3% -> 3% of each run, Pallas kernels for 0% -> 0%
where the time goes in v1:
time: 362 us; the launch traced here: 361 us
  blocking collectives  195 us (54%)
  local copies, waits for them, and re-layouts  63.4 us (18%)
  waiting for transfers between devices  44 us (12%)
  starting transfers between devices  25 us (7%)
  other arithmetic  19.7 us (5%)
  matrix products  13.4 us (4%)
    all_to_all x1, blocking collectives, body(): lax.all_to_all(split_quarters(partial_value, tp_count), 'tp', split_axis=...  72.3 us
    all_to_all x1, blocking collectives, body(): lax.all_to_all(jnp.stack([arrived_own] * lax.axis_size('tp')), 'tp', 0, 0)  72.2 us
    all_to_all x1, blocking collectives, body(): lax.all_to_all(outgoing, 'sp', split_axis=0, concat_axis=0, tiled=True)  50.4 us
    all_to_all x1, waiting for transfers between devices, body(): lax.all_to_all(summed, 'sp', split_axis=0, concat_axis=0, tiled=True)  38.9 us
    another operation x2, local copies, waits for them, and re-layouts, apply_experts(): rows = arrived[:, local].reshape(-1, arrived.shape[3])  12.6 us
    slice x3, local copies, waits for them, and re-layouts, apply_experts(): rows = arrived[:, local].reshape(-1, arrived.shape[3])  11.6 us
    all_to_all x1, starting transfers between devices, body(): lax.all_to_all(summed, 'sp', split_axis=0, concat_axis=0, tiled=True)  10.8 us
    ppermute x3, starting transfers between devices, passed_along(): return lax.ppermute(x, axis, pairs)  10.1 us
  transfers between devices with their start and end apart: 5, of which 2 were waited for; matrix products, arithmetic and copies ran while one was open for 3% of the time, Pallas kernels for 0%

profile of v1, /device:TPU:1, one launch (start us, length us, event | category | flops | bytes accessed | tf_op | source)
XLA Modules:
  0.0 361.0 jit_solution(17213025763822567921)
XLA Ops:
  0.0 0.9 slice.325
  0.9 4.6 %collective-permute-start.2 = (s32[30]{0:T(128)S(1)}, s32[30]{0:T(128)S(1)}, u32[]{:S(2)}, u32[]{:S(2)}) collective-permute-start(s32[30]{0:T(128)S(1)} %slice.325), channel_id=1, source_target_pairs={{0,4},{4,8},{8,12},{12,16},{16,20},{20,24},{24,28},{28,32},{32,36}... | collective-permute-start | bytes 368 | tf_op jit(solution)/shard_map/ppermute | solution.py:12
  5.5 0.7 slice.321
  6.2 1.9 collective-permute-start
  8.1 0.7 slice.322
  8.8 3.6 collective-permute-start.1
  12.4 1.0 slice_bitcast_fusion.31
  13.4 1.0 slice_bitcast_fusion.30
  14.4 0.8 copy.46
  15.2 0.1 eq.149
  15.3 0.1 eq.145
  15.4 0.7 broadcast_multiply_fusion
  16.2 0.2 fusion.88
  16.7 0.1 mul.522
  16.8 0.2 fusion.90
  17.0 1.4 scatter_custom_fusion
  18.4 0.8 pad_add_fusion
  19.2 0.8 slice_compare_fusion.29
  20.0 0.8 slice_compare_fusion.28
  20.8 1.1 divide_multiply_fusion
  21.9 4.1 %fusion.25 = bf16[512,128]{1,0:T(8,128)(2,1)} fusion(f32[542,128]{1,0:T(8,128)S(1)} %divide_multiply_fusion, f32[128]{0:T(128)S(1)} %get-tuple-element.38, f32[128]{0:T(128)S(1)} %get-tuple-element.39, f32[128]{0:T(128)S(1)} %get-tuple-element.10, f32[128]{0:T(128)S(1)} %get-tuple-element.11, f32[128]{0:T(128)S(1)} %get-tuple-element.12, ...), kind=kLoop, calls=%fused_computation.43 | loop fusion | flops 6094848 | bytes 8289280 | tf_op jit(solution)/shard_map/convert_element_type | solution.py:27
  26.0 4.1 %all-to-all-start = ((bf16[4,128,128]{2,1,0:T(8,128)(2,1)}), bf16[4,128,128]{2,1,0:T(8,128)(2,1)S(1)}, u32[]{:S(2)}, u32[]{:S(2)}) async-start(bf16[4,128,128]{2,1,0:T(8,128)(2,1)} %bitcast.31), calls=%async_computation | async-start | bytes 262144 | tf_op jit(solution)/shard_map/all_to_all | solution.py:82
  30.1 5.1 %all-to-all-done = bf16[4,128,128]{2,1,0:T(8,128)(2,1)S(1)} async-done(((bf16[4,128,128]{2,1,0:T(8,128)(2,1)}), bf16[4,128,128]{2,1,0:T(8,128)(2,1)S(1)}, u32[]{:S(2)}, u32[]{:S(2)}) %all-to-all-start) | async-done | bytes 131104 | tf_op jit(solution)/shard_map/all_to_all | solution.py:82
  35.2 0.1 copy.43
  35.4 0.1 convert_reduce_fusion
  35.5 0.2 multiply_convert_fusion.1
  35.7 1.6 multiply_reduce_fusion.1
  37.4 0.2 multiply_convert_fusion
  37.6 3.1 gather_fusion
  40.7 4.0 %reshape.169 = bf16[64,2,3,2048]{3,2,1,0:T(4,128)(2,1)S(1)} reshape(bf16[384,2048]{1,0:T(8,128)(2,1)} %gather_fusion) | data formatting | bytes 3145728 | tf_op jit(solution)/shard_map/reshape | solution.py:112
  44.7 2.1 copy.50
  46.8 50.4 %all_to_all.33 = bf16[64,2,3,2048]{3,1,2,0:T(2,128)(2,1)S(1)} all-to-all(bf16[64,2,3,2048]{3,1,2,0:T(2,128)(2,1)S(1)} %copy.50), channel_id=1, replica_groups=mesh['sp'=64,'tp'=4] {'sp'}, dimensions={0} | all-to-all | bytes 3145728 | tf_op jit(solution)/shard_map/all_to_all | solution.py:113
  97.2 0.6 copy.51
  97.8 0.8 stack.22
  98.7 72.2 %all_to_all.34 = bf16[4,64,2,3,2048]{4,1,3,2,0:T(8,128)(2,1)S(1)} all-to-all(bf16[4,64,2,3,2048]{4,1,3,2,0:T(8,128)(2,1)S(1)} %stack.22), channel_id=1, replica_groups=mesh['sp'=64,'tp'=4] {'tp'}, dimensions={0} | all-to-all | bytes 12582912 | tf_op jit(solution)/shard_map/all_to_all | solution.py:115
  170.9 1.1 copy.52
  172.0 2.3 fusion.97
  174.3 3.7 %copy.53 = bf16[64,1,12,2048]{3,2,0,1:T(8,128)(2,1)} copy(bf16[64,1,12,2048]{3,0,2,1:T(8,128)(2,1)S(1)} %get-tuple-element.7) | data formatting | bytes 6291456 | tf_op jit(solution)/shard_map/slice | solution.py:39
  178.0 6.3 %reshape_squeeze.6 = bf16[768,2048]{1,0:T(8,128)(2,1)} reshape(bf16[64,1,12,2048]{3,2,0,1:T(8,128)(2,1)} %copy.53) | data formatting | bytes 6291456 | tf_op jit(solution)/shard_map/reshape;squeeze | solution.py:39
  184.3 3.0 fusion.12
  187.3 0.4 copy-done.13
  187.8 1.0 fusion.4
  188.8 1.0 reshape.172
  189.7 5.6 %copy.55 = bf16[64,1,12,2048]{3,2,0,1:T(8,128)(2,1)} copy(bf16[64,1,12,2048]{3,0,2,1:T(8,128)(2,1)} %get-tuple-element.8) | data formatting | bytes 6291456 | tf_op jit(solution)/shard_map/slice | solution.py:39
  195.4 6.3 %reshape_squeeze.7 = bf16[768,2048]{1,0:T(8,128)(2,1)} reshape(bf16[64,1,12,2048]{3,2,0,1:T(8,128)(2,1)} %copy.55) | data formatting | bytes 6291456 | tf_op jit(solution)/shard_map/reshape;squeeze | solution.py:39
  201.7 3.0 fusion.9
  204.7 0.4 copy-done.14
  205.2 1.7 fusion.5
  206.9 2.1 reshape.173
  209.0 2.1 fusion
  211.1 1.0 fusion.1
  212.1 0.6 pad_maximum_fusion
  212.7 1.1 copy.57
  213.8 72.3 %all_to_all.35 = bf16[64,2,4,3,2048]{4,0,3,1,2:T(8,128)(2,1)} all-to-all(bf16[64,2,4,3,2048]{4,0,3,1,2:T(8,128)(2,1)S(1)} %copy.57), channel_id=1, replica_groups=mesh['sp'=64,'tp'=4] {'tp'}, dimensions={2} | all-to-all | bytes 12582912 | tf_op jit(solution)/shard_map/all_to_all | solution.py:118
  286.1 4.2 %reduce_sum.64 = bf16[64,2,3,2048]{3,0,2,1:T(8,128)(2,1)S(1)} reduce(bf16[64,2,4,3,2048]{4,0,3,1,2:T(8,128)(2,1)} %all_to_all.35, bf16[]{:T(256)} %constant.46.clone.1), dimensions={2}, to_apply=%region_7.8 | reduce | flops 2359296 | bytes 7864322 | tf_op jit(solution)/shard_map/reduce_sum | solution.py:121
  290.3 2.8 copy.59
  293.1 10.8 %all-to-all-start.4 = ((bf16[64,2,3,2048]{3,1,2,0:T(2,128)(2,1)}), bf16[64,2,3,2048]{3,1,2,0:T(2,128)(2,1)S(1)}, u32[]{:S(2)}, u32[]{:S(2)}) async-start(bf16[64,2,3,2048]{3,1,2,0:T(2,128)(2,1)} %copy.59), calls=%async_computation.4 | async-start | bytes 3145728 | tf_op jit(solution)/shard_map/all_to_all | solution.py:122
  304.1 38.9 %all-to-all-done.4 = bf16[64,2,3,2048]{3,1,2,0:T(2,128)(2,1)S(1)} async-done(((bf16[64,2,3,2048]{3,1,2,0:T(2,128)(2,1)}), bf16[64,2,3,2048]{3,1,2,0:T(2,128)(2,1)S(1)}, u32[]{:S(2)}, u32[]{:S(2)}) %all-to-all-start.4) | async-done | bytes 1572896 | tf_op jit(solution)/shard_map/all_to_all | solution.py:122
  343.0 2.4 copy.60
  345.4 3.9 %reshape.174 = bf16[384,2048]{1,0:T(8,128)(2,1)S(1)} reshape(bf16[64,2,3,2048]{3,2,1,0:T(4,128)(2,1)} %copy.60) | data formatting | bytes 3145728 | tf_op jit(solution)/shard_map/reshape | solution.py:123
  349.3 2.3 gather_fusion.1
  351.7 3.5 reshape.178
  355.2 4.8 %multiply_reduce_fusion = f32[128,2048]{1,0:T(8,128)S(1)} fusion(f32[128,2,2048]{2,1,0:T(2,128)} %reshape.178, f32[128,2]{1,0:T(8,128)S(1)} %copy.44), kind=kLoop, calls=%fused_computation.11 | loop fusion | flops 786432 | bytes 3146752 | tf_op jit(solution)/shard_map/reduce_sum | solution.py:125
  360.0 0.9 add_convert_fusion
  (51 shorter events, 0.6 us)
Async XLA Ops:
  0.0 35.7 %copy-start = (bf16[512,2048]{1,0:T(8,128)(2,1)S(1)}, bf16[512,2048]{1,0:T(8,128)(2,1)}, u32[]{:S(2)}) copy-start(bf16[512,2048]{1,0:T(8,128)(2,1)} %param.24) | copy-start | bytes 6291460
  0.9 17.5 %collective-permute-start.2 = (s32[30]{0:T(128)S(1)}, s32[30]{0:T(128)S(1)}, u32[]{:S(2)}, u32[]{:S(2)}) collective-permute-start(s32[30]{0:T(128)S(1)} %slice.325), channel_id=1, source_target_pairs={{0,4},{4,8},{8,12},{12,16},{16,20},{20,24},{24,28},{28,32},{32,36}... | collective-permute-start | bytes 368 | tf_op jit(solution)/shard_map/ppermute | solution.py:12
  6.2 14.5 %collective-permute-start = (bf16[30,128]{1,0:T(8,128)(2,1)S(1)}, bf16[30,128]{1,0:T(8,128)(2,1)S(1)}, u32[]{:S(2)}, u32[]{:S(2)}) collective-permute-start(bf16[30,128]{1,0:T(8,128)(2,1)S(1)} %slice.321), channel_id=1, source_target_pairs={{0,4},{4,8},{8,12},{12,16},{16,20},{20,24},{24,28},{28,32},{32,36}... | collective-permute-start | bytes 23048 | tf_op jit(solution)/shard_map/ppermute | solution.py:12
  8.8 11.9 %collective-permute-start.1 = (bf16[30,128]{1,0:T(8,128)(2,1)S(1)}, bf16[30,128]{1,0:T(8,128)(2,1)S(1)}, u32[]{:S(2)}, u32[]{:S(2)}) collective-permute-start(bf16[30,128]{1,0:T(8,128)(2,1)S(1)} %slice.322), channel_id=1, source_target_pairs={{0,4},{4,8},{8,12},{12,16},{16,20},{20,24},{24,28},{28,32},{32,36}... | collective-permute-start | bytes 23048 | tf_op jit(solution)/shard_map/ppermute | solution.py:12
  21.8 13.7 %copy-start.7 = (f32[512]{0:T(512)S(1)}, f32[512]{0:T(512)}, u32[]{:S(2)}) copy-start(f32[512]{0:T(512)} %param.23) | copy-start | bytes 6148
  21.8 13.7 %copy-start.8 = (f32[512]{0:T(512)S(1)}, f32[512]{0:T(512)}, u32[]{:S(2)}) copy-start(f32[512]{0:T(512)} %param.22) | copy-start | bytes 6148
  26.0 11.4 %copy-start.6 = (f32[2048]{0:T(1024)S(1)}, f32[2048]{0:T(1024)}, u32[]{:S(2)}) copy-start(f32[2048]{0:T(1024)} %param.25) | copy-start | bytes 24580
  26.0 9.2 %all-to-all-start = ((bf16[4,128,128]{2,1,0:T(8,128)(2,1)}), bf16[4,128,128]{2,1,0:T(8,128)(2,1)S(1)}, u32[]{:S(2)}, u32[]{:S(2)}) async-start(bf16[4,128,128]{2,1,0:T(8,128)(2,1)} %bitcast.31), calls=%async_computation | async-start | bytes 262144 | tf_op jit(solution)/shard_map/all_to_all | solution.py:82
  178.0 6.3 %copy-start.11 = (bf16[2,2048,256]{2,1,0:T(8,128)(2,1)S(1)}, bf16[2,2048,256]{2,1,0:T(8,128)(2,1)}, u32[]{:S(2)}) copy-start(bf16[2,2048,256]{2,1,0:T(8,128)(2,1)} %param.29) | copy-start | bytes 6291460
  184.3 3.0 copy-start.2
  184.3 3.5 copy-start.13
  195.3 6.3 %copy-start.12 = (bf16[2,2048,256]{2,1,0:T(8,128)(2,1)S(1)}, bf16[2,2048,256]{2,1,0:T(8,128)(2,1)}, u32[]{:S(2)}) copy-start(bf16[2,2048,256]{2,1,0:T(8,128)(2,1)} %param.29) | copy-start | bytes 6291460
  201.7 3.0 copy-start.3
  201.7 3.5 copy-start.14
  205.2 3.8 %copy-start.4 = (bf16[2,256,2048]{2,1,0:T(8,128)(2,1)S(1)}, bf16[2,256,2048]{2,1,0:T(8,128)(2,1)}, u32[]{:S(2)}) copy-start(bf16[2,256,2048]{2,1,0:T(8,128)(2,1)} %param.31) | copy-start | bytes 6291460
  209.0 2.1 copy-start.5
  290.3 13.6 %copy-start.9 = (f32[128,2]{0,1:T(2,128)S(1)}, f32[128,2]{0,1:T(2,128)}, u32[]{:S(2)}) copy-start(f32[128,2]{0,1:T(2,128)} %param.28) | copy-start | bytes 3076
  290.3 13.6 %copy-start.10 = (f32[128]{0:T(128)S(1)}, f32[128]{0:T(128)}, u32[]{:S(2)}) copy-start(f32[128]{0:T(128)} %param.27) | copy-start | bytes 1540
  293.1 49.9 %all-to-all-start.4 = ((bf16[64,2,3,2048]{3,1,2,0:T(2,128)(2,1)}), bf16[64,2,3,2048]{3,1,2,0:T(2,128)(2,1)S(1)}, u32[]{:S(2)}, u32[]{:S(2)}) async-start(bf16[64,2,3,2048]{3,1,2,0:T(2,128)(2,1)} %copy.59), calls=%async_computation.4 | async-start | bytes 3145728 | tf_op jit(solution)/shard_map/all_to_all | solution.py:122
  351.7 9.3 %copy-start.1 = (bf16[512,2048]{1,0:T(8,128)(2,1)S(1)}, bf16[512,2048]{1,0:T(8,128)(2,1)}, u32[]{:S(2)}) copy-start(bf16[512,2048]{1,0:T(8,128)(2,1)} %param.24) | copy-start | bytes 6291460
